TPU v7x, 32 devices: a whole 2x2x4 slice. The times are simulated.
32 devices in a mesh: rep: 2 (over y), fs: 4 (over z), tp: 4 (over x, core).
Axes of the slice: x: 2, y: 2, z: 4, core: 2. Of those that a mesh axis runs over, the one named last changes fastest.
Arguments:
- tokens: bfloat16 [4096, 2048], P(('rep', 'fs', 'tp')), may hold values from -6 to 6
- norm_gain: float32 [2048], replicated, may hold values from 0.1 to 1.9
- w_gate: bfloat16 [2048, 3072], P('fs', 'tp'), may hold values from -0.125 to 0.125
- w_up: bfloat16 [2048, 3072], P('fs', 'tp'), may hold values from -0.125 to 0.125
- w_down: bfloat16 [3072, 2048], P('tp', 'fs'), may hold values from -0.109375 to 0.109375
- post_gain: float32 [2048], replicated, may hold values from 0.1 to 1.9
Outputs:
- result: bfloat16 [4096, 2048], P(('rep', 'fs', 'tp'))
All inputs are finite; a program needn't handle non-finite values.
Results may differ from a plain program's by a relative error of at most 0.014.
Values may be sent and summed in bfloat16 or wider, within the bound.
A program may use at most 64 MiB of HBM per device.

v0:
```python
import jax
import jax.numpy as jnp
from jax import lax
from jax.sharding import PartitionSpec as P

EPS = 1e-06


def rms_scale(values, gain):
    return values * lax.rsqrt(jnp.mean(values * values, axis=-1, keepdims=True) + EPS) * gain


def body(tokens, norm_gain, w_gate, w_up, w_down, post_gain):
    own_normed = rms_scale(tokens.astype(jnp.float32), norm_gain).astype(jnp.bfloat16)
    normed = lax.all_gather(own_normed, "tp", axis=0, tiled=True)
    gate = jnp.dot(
        normed, lax.all_gather(w_gate, "fs", axis=0, tiled=True), preferred_element_type=jnp.float32
    )
    up = jnp.dot(
        normed, lax.all_gather(w_up, "fs", axis=0, tiled=True), preferred_element_type=jnp.float32
    )
    hidden = (jax.nn.silu(gate) * up).astype(jnp.bfloat16)
    terms = jnp.dot(
        hidden, lax.all_gather(w_down, "fs", axis=1, tiled=True), preferred_element_type=jnp.float32
    )
    summed = lax.psum_scatter(
        terms.astype(jnp.bfloat16), "tp", scatter_dimension=0, tiled=True
    ).astype(jnp.float32)
    return rms_scale(summed, post_gain).astype(jnp.bfloat16)


def solution(mesh):
    return jax.shard_map(
        body,
        mesh=mesh,
        in_specs=(
            P(("rep", "fs", "tp"), None),
            P(),
            P("fs", "tp"),
            P("fs", "tp"),
            P("tp", "fs"),
            P(),
        ),
        out_specs=P(("rep", "fs", "tp"), None),
        check_vma=False,
    )
```

profile of v0, /device:TPU:0, one launch (start us, length us, event | category | flops | bytes accessed | tf_op | source)
XLA Modules:
  0.0 276.0 jit_solution(9713884520916390494)
XLA Ops:
  6.5 0.0 all-gather.5.cloned.1.call-start
  6.5 1.2 fusion
  7.8 2.0 fusion.2
  9.8 0.0 all-gather.5.cloned.1.call-update
  9.8 0.0 all-gather.7.cloned.1.call-start
  9.9 0.7 all-gather.7.cloned.1.call-update
  10.6 0.0 all-gather.11.cloned.1.call-start
  10.6 0.7 all-gather.11.cloned.1.call-update
  11.3 0.0 all-gather.9.cloned.1.call-start
  11.4 0.5 all-gather.9.cloned.1.call-update
  11.9 0.0 reduce-scatter.2.cloned.1.call-start
  11.9 23.3 %all-gather.5.cloned.1.call-done = bf16[512,2048]{1,0:T(8,128)(2,1)} async-done(((bf16[128,2048]{1,0:T(8,128)(2,1)}), bf16[512,2048]{1,0:T(8,128)(2,1)}) %all-gather.5.cloned.1.call-update) | async-done | bytes 2097168 | tf_op jit(solution)/shard_map/all_gather | solution.py:15
  35.3 0.0 copy-start.1
  35.3 65.0 %all-gather.7.cloned.1.call-done = bf16[2048,768]{1,0:T(8,128)(2,1)} async-done(((bf16[512,768]{1,0:T(8,128)(2,1)}), bf16[2048,768]{1,0:T(8,128)(2,1)}) %all-gather.7.cloned.1.call-update) | async-done | bytes 3145744 | tf_op jit(solution)/shard_map/all_gather | solution.py:17
  100.3 5.5 %fusion.7 = f32[512,768]{1,0:T(8,128)} fusion(bf16[512,2048]{1,0:T(8,128)(2,1)} %all-gather.5.cloned.1.call-done, bf16[2048,768]{1,0:T(8,128)(2,1)} %all-gather.7.cloned.1.call-done), kind=kOutput, calls=%fused_computation.15 | convolution fusion | flops 1610612736 | bytes 6815744 | tf_op jit(solution)/shard_map/dot_general | solution.py:16
  105.8 58.2 %all-gather.11.cloned.1.call-done = bf16[768,2048]{1,0:T(8,128)(2,1)} async-done(((bf16[768,512]{1,0:T(8,128)(2,1)}), bf16[768,2048]{1,0:T(8,128)(2,1)}) %all-gather.11.cloned.1.call-update) | async-done | bytes 3145744 | tf_op jit(solution)/shard_map/all_gather | solution.py:24
  164.0 63.5 %all-gather.9.cloned.1.call-done = bf16[2048,768]{1,0:T(8,128)(2,1)} async-done(((bf16[512,768]{1,0:T(8,128)(2,1)}), bf16[2048,768]{1,0:T(8,128)(2,1)}) %all-gather.9.cloned.1.call-update) | async-done | bytes 3145744 | tf_op jit(solution)/shard_map/all_gather | solution.py:20
  227.5 0.0 copy-done.1
  227.6 8.6 %convolution_convert_fusion = bf16[512,2048]{1,0:T(8,128)(2,1)} fusion(bf16[768,2048]{1,0:T(8,128)(2,1)} %all-gather.11.cloned.1.call-done, f32[512,768]{1,0:T(8,128)} %fusion.7, bf16[512,2048]{1,0:T(8,128)(2,1)S(1)} %copy-done.1, bf16[2048,768]{1,0:T(8,128)(2,1)} %all-gather.9.cloned.1.call-done), kind=kOutput, calls=%fused_computation | convolution fusion | flops 3224633344 | bytes 12058624 | tf_op jit(solution)/shard_map/dot_general | solution.py:23
  236.2 0.0 reduce-scatter.2.cloned.1.call-update
  236.2 30.0 %reduce-scatter.2.cloned.1.call-done = bf16[128,2048]{1,0:T(8,128)(2,1)} async-done(((bf16[512,2048]{1,0:T(8,128)(2,1)}), bf16[128,2048]{1,0:T(8,128)(2,1)}) %reduce-scatter.2.cloned.1.call-update) | async-done | bytes 524304 | tf_op jit(solution)/shard_map/reduce_scatter | solution.py:26
  266.2 1.2 fusion.3
  267.4 0.0 copy-done
  267.4 2.0 fusion.5
  (3 shorter events, 0.0 us)
Async XLA Ops:
  6.5 28.7 %all-gather.5.cloned.1.call-start = ((), (), s32[]{:S(2)}) async-start(), calls=%async_computation.1 | async-start | bytes 2621440 | tf_op jit(solution)/shard_map/all_gather | solution.py:15
  9.8 90.5 %all-gather.7.cloned.1.call-start = ((), (), s32[]{:S(2)}) async-start(), calls=%async_computation.2 | async-start | bytes 3932160 | tf_op jit(solution)/shard_map/all_gather | solution.py:17
  10.6 153.4 %all-gather.11.cloned.1.call-start = ((), (), s32[]{:S(2)}) async-start(), calls=%async_computation.4 | async-start | bytes 3932160 | tf_op jit(solution)/shard_map/all_gather | solution.py:24
  11.3 216.2 %all-gather.9.cloned.1.call-start = ((), (), s32[]{:S(2)}) async-start(), calls=%async_computation.3 | async-start | bytes 3932160 | tf_op jit(solution)/shard_map/all_gather | solution.py:20
  11.9 254.3 %reduce-scatter.2.cloned.1.call-start = ((), (), s32[]{:S(2)}) async-start(), calls=%async_computation.5 | async-start | bytes 2621440 | tf_op jit(solution)/shard_map/reduce_scatter | solution.py:26
  35.3 192.3 %copy-start.1 = (bf16[512,2048]{1,0:T(8,128)(2,1)S(1)}, bf16[512,2048]{1,0:T(8,128)(2,1)}, u32[]{:S(2)}) copy-start(bf16[512,2048]{1,0:T(8,128)(2,1)} %all-gather.5.cloned.1.call-done) | copy-start | bytes 6291460
  236.2 31.2 %copy-start = (f32[2048]{0:T(1024)S(1)}, f32[2048]{0:T(1024)}, u32[]{:S(2)}) copy-start(f32[2048]{0:T(1024)} %param.11) | copy-start | bytes 24580
Sparse Core Ops, SparseCore 0:
  9.9 25.2 all-gather.4
  36.8 63.4 all-gather.6
  101.9 62.0 all-gather.10
  165.4 62.0 all-gather.8
  236.3 29.7 reduce-scatter.1
where the time goes:
time: 276 us
  waiting for transfers between devices  242 us (88%)
  matrix products  14.1 us (5%)
  between operations  13.1 us (5%)
  other arithmetic  6.53 us (2%)
    all_gather x1, waiting for transfers between devices, body(): lax.all_gather(w_gate, 'fs', axis=0, tiled=True)  65 us
    all_gather x1, waiting for transfers between devices, body(): lax.all_gather(w_up, 'fs', axis=0, tiled=True)  63.5 us
    all_gather x1, waiting for transfers between devices, body(): lax.all_gather(w_down, 'fs', axis=1, tiled=True)  58.2 us
    reduce_scatter x1, waiting for transfers between devices, body(): lax.psum_scatter(terms.astype(jnp.bfloat16), 'tp', scatter_dimension=0, t...  30 us
    all_gather x1, waiting for transfers between devices, body(): normed = lax.all_gather(own_normed, 'tp', axis=0, tiled=True)  23.3 us
    dot_general x1, matrix products, body(): jnp.dot(hidden, lax.all_gather(w_down, 'fs', axis=1, tiled=True), preferr...  8.63 us
  transfers between devices with their start and end apart: 5, of which 5 were waited for; matrix products, arithmetic and copies ran while one was open for 2% of the time, Pallas kernels for 0%

commit v1 on v0

--- a/solution.py
+++ b/solution.py
@@ -1,16 +1,21 @@
+import functools
+
 import jax
 import jax.numpy as jnp
 from jax import lax
+from jax.experimental import pallas as pl
+from jax.experimental.pallas import tpu as pltpu
 from jax.sharding import PartitionSpec as P
 
 EPS = 1e-06
+MESH = pl.DeviceIdType.MESH
 
 
 def rms_scale(values, gain):
     return values * lax.rsqrt(jnp.mean(values * values, axis=-1, keepdims=True) + EPS) * gain
 
 
-def body(tokens, norm_gain, w_gate, w_up, w_down, post_gain):
+def plain_body(tokens, norm_gain, w_gate, w_up, w_down, post_gain):
     own_normed = rms_scale(tokens.astype(jnp.float32), norm_gain).astype(jnp.bfloat16)
     normed = lax.all_gather(own_normed, "tp", axis=0, tiled=True)
     gate = jnp.dot(
@@ -29,7 +34,289 @@
     return rms_scale(summed, post_gain).astype(jnp.bfloat16)
 
 
+def kernel(
+    n, rows, depth, part, width,
+    tok_ref, gain_ref, wg_ref, wu_ref, wd_ref, post_ref, out_ref,
+    raw, normed, gu, dn, hidden, kept, pair_out, pair_in, cross_out, cross_in, fin,
+    loc_sem, tok_s, tok_r, w_s, w_r, pair_s, pair_r, cross_s, cross_r,
+):
+    r, k, t = lax.axis_index("rep"), lax.axis_index("fs"), lax.axis_index("tp")
+    x, c = t // 2, t % 2
+    t_pair, t_x, r_y = x * 2 + (1 - c), (1 - x) * 2 + c, 1 - r
+    partner, along_x, along_y, diag = {"tp": t_pair}, {"tp": t_x}, {"rep": r_y}, {"rep": r_y, "tp": t_x}
+    has_left, has_right = k > 0, k < n - 1
+
+    def weight(s, q):
+        if q < 2:
+            return gu.at[pl.ds(s * depth, depth), pl.ds(q * part, part)]
+        return dn.at[s]
+
+    half = pl.multiple_of(r * part, part)
+    loads = [
+        pltpu.make_async_copy(wg_ref.at[:, pl.ds(half, part)], weight(k, 0), loc_sem.at[0]),
+        pltpu.make_async_copy(wu_ref.at[:, pl.ds(half, part)], weight(k, 1), loc_sem.at[1]),
+        pltpu.make_async_copy(wd_ref.at[pl.ds(half, part), :], weight(k, 2), loc_sem.at[2]),
+        pltpu.make_async_copy(tok_ref, raw.at[pl.ds((r * 4 + t) * rows, rows)], loc_sem.at[3]),
+    ]
+    for load in loads:
+        load.start()
+
+    barrier = pltpu.get_barrier_semaphore()
+    for where in (partner, along_x, along_y, diag):
+        pl.semaphore_signal(barrier, inc=1, device_id=where, device_id_type=MESH)
+
+    @pl.when(has_left)
+    def _():
+        pl.semaphore_signal(barrier, inc=1, device_id={"fs": k - 1}, device_id_type=MESH)
+
+    @pl.when(has_right)
+    def _():
+        pl.semaphore_signal(barrier, inc=1, device_id={"fs": k + 1}, device_id_type=MESH)
+
+    pl.semaphore_wait(barrier, 4 + jnp.where(has_left, 1, 0) + jnp.where(has_right, 1, 0))
+
+    def remote(ref, send, recv, where):
+        return pltpu.make_async_remote_copy(ref, ref, send, recv, device_id=where, device_id_type=MESH)
+
+    def hop(way, s, q):
+        return remote(weight(s, q), w_s.at[way, s, q], w_r.at[s, q], {"fs": k + 1 - 2 * way})
+
+    def pass_on(way, s, q):
+        @pl.when(has_left if way else has_right)
+        def _():
+            hop(way, s, q).start()
+
+    def rows_of(r_at, t_at, first=0, count=rows):
+        return raw.at[pl.ds((r_at * 4 + t_at) * rows + first, count)]
+
+    upper = rows // 2
+    token_sends = [
+        (rows_of(r, t), partner),
+        (rows_of(r, t), along_x),
+        (rows_of(r, t), along_y),
+        (rows_of(r, t_x, 0, upper), along_y),
+        (rows_of(r_y, t, upper, upper), along_x),
+        (rows_of(r, t_x), partner),
+        (rows_of(r_y, t), partner),
+        (rows_of(r_y, t_x), partner),
+    ]
+    t_px = (1 - x) * 2 + (1 - c)
+    token_lands = [
+        rows_of(r, t_pair),
+        rows_of(r, t_x),
+        rows_of(r_y, t),
+        rows_of(r_y, t_x, 0, upper),
+        rows_of(r_y, t_x, upper, upper),
+        rows_of(r, t_px),
+        rows_of(r_y, t_pair),
+        rows_of(r_y, t_px),
+    ]
+
+    def token_send(i):
+        ref, where = token_sends[i]
+        return remote(ref, tok_s.at[i], tok_r.at[i], where)
+
+    def token_wait(i):
+        remote(token_lands[i], tok_s.at[i], tok_r.at[i], partner).wait_recv()
+
+    loads[3].wait()
+    for i in (1, 2, 0):
+        token_send(i).start()
+    for q in (0, 1):
+        loads[q].wait()
+        pass_on(0, k, q)
+        pass_on(1, k, q)
+
+    def arrive(step, q):
+        for way, s in ((0, k - step), (1, k + step)):
+            @pl.when((s >= 0) if way == 0 else (s < n))
+            def _():
+                hop(way, s, q).wait_recv()
+                pass_on(way, s, q)
+
+    def forward_tokens():
+        token_wait(1)
+        token_send(3).start()
+        token_send(5).start()
+        token_wait(2)
+        token_send(4).start()
+        token_send(6).start()
+
+    def finish_tokens():
+        token_wait(3)
+        token_wait(4)
+        token_send(7).start()
+        for i in (0, 5, 6, 7):
+            token_wait(i)
+
+        tile = 32
+
+        @pl.loop(0, 8 * rows // tile)
+        def _(i):
+            at = pl.ds(pl.multiple_of(i * tile, tile), tile)
+            normed[at, :] = rms_scale(raw[at, :].astype(jnp.float32), gain_ref[...]).astype(jnp.bfloat16)
+
+    for step in range(1, n):
+        arrive(step, 0)
+        if step == 1:
+            forward_tokens()
+        arrive(step, 1)
+        if step == 1:
+            finish_tokens()
+
+    loads[2].wait()
+    pass_on(0, k, 2)
+    pass_on(1, k, 2)
+
+    tile = 2 * rows
+
+    @pl.loop(0, 4)
+    def _(i):
+        at = pl.ds(pl.multiple_of(i * tile, tile), tile)
+        both = jnp.dot(normed[at, :], gu[...], preferred_element_type=jnp.float32)
+        gate, up = both[:, :part], both[:, part:]
+        hidden[at, :] = (gate / (1.0 + jnp.exp(-gate)) * up).astype(jnp.bfloat16)
+
+    mine = r * 2 + x
+    others = ((r * 2 + (1 - x), along_x), (r_y * 2 + x, along_y), (r_y * 2 + (1 - x), diag))
+
+    def pair_copy(s):
+        return pltpu.make_async_remote_copy(
+            pair_out.at[s], pair_in.at[s], pair_s.at[s], pair_r.at[s], device_id=partner, device_id_type=MESH
+        )
+
+    def cross_copy(s, to, where):
+        return pltpu.make_async_remote_copy(
+            cross_out.at[s, to], cross_in.at[s, mine], cross_s.at[s, to], cross_r.at[s, mine],
+            device_id=where, device_id_type=MESH,
+        )
+
+    def reduce_block(s):
+        @pl.loop(0, 4)
+        def _(m):
+            at = pl.ds(pl.multiple_of((m * 2 + (1 - c)) * rows, rows), rows)
+            pair_out[s, m] = jnp.dot(
+                hidden[at, :], dn[s], preferred_element_type=jnp.float32
+            ).astype(jnp.bfloat16)
+
+        pair_copy(s).start()
+
+        @pl.loop(0, 4)
+        def _(m):
+            at = pl.ds(pl.multiple_of((m * 2 + c) * rows, rows), rows)
+            kept[m] = jnp.dot(hidden[at, :], dn[s], preferred_element_type=jnp.float32)
+
+        pair_copy(s).wait_recv()
+        for to, where in others:
+            cross_out[s, to] = (kept[to] + pair_in[s, to].astype(jnp.float32)).astype(jnp.bfloat16)
+        for to, where in (others[2], others[0], others[1]):
+            cross_copy(s, to, where).start()
+        fin[s] = kept[mine] + pair_in[s, mine].astype(jnp.float32)
+
+    reduce_block(k)
+    for step in range(1, n):
+        arrive(step, 2)
+        for s in (k - step, k + step):
+            @pl.when((s >= 0) & (s < n))
+            def _():
+                reduce_block(s)
+
+    def take(i):
+        for s_at in range(n):
+            for other, _ in others:
+                pltpu.make_async_remote_copy(
+                    cross_out.at[s_at, 0], cross_in.at[s_at, other], cross_s.at[s_at, 0],
+                    cross_r.at[s_at, other], device_id=along_x, device_id_type=MESH,
+                ).wait_recv()
+
+    take(0)
+    piece = 32
+
+    @pl.loop(0, rows // piece)
+    def _(i):
+        at = pl.ds(pl.multiple_of(i * piece, piece), piece)
+        blocks = []
+        for s in range(n):
+            total = fin[s, at, :]
+            for other, _ in others:
+                total = total + cross_in[s, other, at, :].astype(jnp.float32)
+            blocks.append(total)
+        square = sum(jnp.sum(b * b, axis=-1, keepdims=True) for b in blocks)
+        scale = lax.rsqrt(square / (n * width) + EPS)
+        for s in range(n):
+            cols = pl.ds(s * width, width)
+            out_ref[at, cols] = (blocks[s] * scale * post_ref[:, cols]).astype(out_ref.dtype)
+
+    for i in range(8):
+        token_send(i).wait_send()
+    for s in range(n):
+        for q in range(3):
+            @pl.when(has_right & (s <= k))
+            def _():
+                hop(0, s, q).wait_send()
+
+            @pl.when(has_left & (s >= k))
+            def _():
+                hop(1, s, q).wait_send()
+        pair_copy(s).wait_send()
+        for to, where in others:
+            cross_copy(s, to, where).wait_send()
+
+
+def chain_body(n, tokens, norm_gain, w_gate, w_up, w_down, post_gain):
+    rows, model = tokens.shape
+    depth, block = w_gate.shape
+    width = w_down.shape[1]
+    part = block // 2
+    vmem, dma = pltpu.VMEM, pltpu.SemaphoreType.DMA
+    low, full = jnp.bfloat16, jnp.float32
+    anywhere = pl.BlockSpec(memory_space=pl.ANY)
+    inside = pl.BlockSpec(memory_space=vmem)
+    return pl.pallas_call(
+        functools.partial(kernel, n, rows, depth, part, width),
+        out_shape=jax.ShapeDtypeStruct((rows, model), low),
+        in_specs=[anywhere, inside, anywhere, anywhere, anywhere, inside],
+        out_specs=inside,
+        scratch_shapes=[
+            vmem((8 * rows, model), low),
+            vmem((8 * rows, model), low),
+            vmem((n * depth, 2 * part), low),
+            vmem((n, part, width), low),
+            vmem((8 * rows, part), low),
+            vmem((4, rows, width), full),
+            vmem((n, 4, rows, width), low),
+            vmem((n, 4, rows, width), low),
+            vmem((n, 4, rows, width), low),
+            vmem((n, 4, rows, width), low),
+            vmem((n, rows, width), full),
+            dma((4,)),
+            dma((8,)),
+            dma((8,)),
+            dma((2, n, 3)),
+            dma((n, 3)),
+            dma((n,)),
+            dma((n,)),
+            dma((n, 4)),
+            dma((n, 4)),
+        ],
+        compiler_params=pltpu.CompilerParams(
+            collective_id=0, has_side_effects=True, vmem_limit_bytes=56 * 2**20
+        ),
+    )(tokens, norm_gain.reshape(1, -1), w_gate, w_up, w_down, post_gain.reshape(1, -1))
+
+
 def solution(mesh):
+    n = mesh.shape["fs"]
+
+    def body(tokens, norm_gain, w_gate, w_up, w_down, post_gain):
+        args = (tokens, norm_gain, w_gate, w_up, w_down, post_gain)
+        rows = tokens.shape[0]
+        fits = (
+            mesh.shape["rep"] == 2 and mesh.shape["tp"] == 4 and 2 <= n <= 4 and rows <= 128
+            and rows % 64 == 0 and w_gate.shape[1] % 256 == 0 and w_down.shape[1] % 128 == 0
+        )
+        return chain_body(n, *args) if fits else plain_body(*args)
+
     return jax.shard_map(
         body,
         mesh=mesh,

time: 276 us -> 96.8 us (0.35)
  waiting for transfers between devices: 242 us -> 0 us
  Pallas kernels: 0 us -> 94.6 us
  matrix products: 14.1 us -> 0 us
  between operations: 13.1 us -> 0.01 us
  other arithmetic: 6.53 us -> 0 us
    all_gather x4 -> x0, waiting for transfers between devices: 210 us -> none  [the longest x1 65 us: body(): lax.all_gather(w_gate, 'fs', axis=0, tiled=True)]
    pallas_call x0 -> x1, Pallas kernels: none -> 94.6 us  [chain_body(): pl.pallas_call(functools.partial(kernel, n, rows, depth, part, width), ou...]
    reduce_scatter x1 -> x0, waiting for transfers between devices: 30 us -> none  [body(): lax.psum_scatter(terms.astype(jnp.bfloat16), 'tp', scatter_dimension=0, t...]
    dot_general x2 -> x0, matrix products: 14.1 us -> none  [the longest x1 8.63 us: body(): jnp.dot(hidden, lax.all_gather(w_down, 'fs', axis=1, tiled=True), preferr...]
    convert_element_type x2 -> x0, other arithmetic: 4.05 us -> none  [the longest x1 2.03 us: body(): rms_scale(tokens.astype(jnp.float32), norm_gain).astype(jnp.bfloat16)]
  transfers between devices with their start and end apart: 5 -> 0, of which waited for: 5 -> 0; matrix products, arithmetic and copies ran while one was open for 2% -> 0% of each run, Pallas kernels for 0% -> 0%
where the time goes in v1:
time: 96.8 us; the launch traced here: 96.5 us
  Pallas kernels  94.6 us (98%)
  local copies, waits for them, and re-layouts  1.88 us (2%)
    pallas_call x1, Pallas kernels, chain_body(): pl.pallas_call(functools.partial(kernel, n, rows, depth, part, width), ou...  94.6 us

profile of v1, /device:TPU:0, one launch (start us, length us, event | category | flops | bytes accessed | tf_op | source)
XLA Modules:
  0.0 96.5 jit_solution(2669563739447983085)
XLA Ops:
  0.0 94.6 %shard_map.64 = bf16[128,2048]{1,0:T(8,128)(2,1)} custom-call(bf16[128,2048]{1,0:T(8,128)(2,1)} %tok_ref.1, f32[1,2048]{1,0:T(1,128)} %bitcast.2, bf16[512,768]{1,0:T(8,128)(2,1)} %wg_ref.1, bf16[512,768]{1,0:T(8,128)(2,1)} %wu_ref.1, bf16[768,512]{1,0:T(8,128)(2,1)} %wd_ref.1, f32[1,2048]{1,0:T(1,128)} %bitcast.3), custom_call_target="tpu_custom_call" | custom-call | tf_op jit(solution)/shard_map/pallas_call | solution.py:275
  94.6 1.9 %copy.8 = bf16[128,2048]{1,0:T(8,128)(2,1)} copy(bf16[128,2048]{1,0:T(8,128)(2,1)} %shard_map.64) | data formatting | bytes 1048576

commit v2 on v1

--- a/solution.py
+++ b/solution.py
@@ -9,6 +9,7 @@
 
 EPS = 1e-06
 MESH = pl.DeviceIdType.MESH
+PIECE = 256
 
 
 def rms_scale(values, gain):
@@ -35,9 +36,9 @@
 
 
 def kernel(
-    n, rows, depth, part, width,
+    n, rows, depth, part, width, cuts,
     tok_ref, gain_ref, wg_ref, wu_ref, wd_ref, post_ref, out_ref,
-    raw, normed, gu, dn, hidden, kept, pair_out, pair_in, cross_out, cross_in, fin,
+    raw, normed, acc, gu, dn, hidden, kept, pair_out, pair_in, cross_out, cross_in, fin,
     loc_sem, tok_s, tok_r, w_s, w_r, pair_s, pair_r, cross_s, cross_r,
 ):
     r, k, t = lax.axis_index("rep"), lax.axis_index("fs"), lax.axis_index("tp")
@@ -47,16 +48,21 @@
     has_left, has_right = k > 0, k < n - 1
 
     def weight(s, q):
-        if q < 2:
-            return gu.at[pl.ds(s * depth, depth), pl.ds(q * part, part)]
-        return dn.at[s]
-
+        if isinstance(q, int) and q < 2:
+            return gu.at[s, :, pl.ds(q * part, part)]
+        return dn.at[s, q - 2]
+
+    sub = width // cuts
     half = pl.multiple_of(r * part, part)
     loads = [
         pltpu.make_async_copy(wg_ref.at[:, pl.ds(half, part)], weight(k, 0), loc_sem.at[0]),
         pltpu.make_async_copy(wu_ref.at[:, pl.ds(half, part)], weight(k, 1), loc_sem.at[1]),
-        pltpu.make_async_copy(wd_ref.at[pl.ds(half, part), :], weight(k, 2), loc_sem.at[2]),
-        pltpu.make_async_copy(tok_ref, raw.at[pl.ds((r * 4 + t) * rows, rows)], loc_sem.at[3]),
+        pltpu.make_async_copy(tok_ref, raw.at[pl.ds((r * 4 + t) * rows, rows)], loc_sem.at[2]),
+    ] + [
+        pltpu.make_async_copy(
+            wd_ref.at[pl.ds(half, part), pl.ds(j * sub, sub)], dn.at[k, j], loc_sem.at[3 + j]
+        )
+        for j in range(cuts)
     ]
     for load in loads:
         load.start()
@@ -119,13 +125,24 @@
     def token_wait(i):
         remote(token_lands[i], tok_s.at[i], tok_r.at[i], partner).wait_recv()
 
-    loads[3].wait()
+    loads[2].wait()
     for i in (1, 2, 0):
         token_send(i).start()
     for q in (0, 1):
         loads[q].wait()
         pass_on(0, k, q)
         pass_on(1, k, q)
+    for load in loads[3:]:
+        load.wait()
+
+    def start_down(step):
+        for way, distance in ((0, k), (1, n - 1 - k)):
+            @pl.when(distance == step)
+            def _():
+                for j in range(cuts):
+                    pass_on(way, k, 2 + j)
+
+    start_down(0)
 
     def arrive(step, q):
         for way, s in ((0, k - step), (1, k + step)):
@@ -156,101 +173,133 @@
             at = pl.ds(pl.multiple_of(i * tile, tile), tile)
             normed[at, :] = rms_scale(raw[at, :].astype(jnp.float32), gain_ref[...]).astype(jnp.bfloat16)
 
+    tile = 2 * rows
+
+    def add_block(s, first):
+        cols = pl.ds(pl.multiple_of(s * depth, depth), depth)
+
+        @pl.loop(0, 4)
+        def _(i):
+            at = pl.ds(pl.multiple_of(i * tile, tile), tile)
+            term = jnp.dot(normed[at, cols], gu[s], preferred_element_type=jnp.float32)
+            acc[at, :] = term if first else acc[at, :] + term
+
     for step in range(1, n):
         arrive(step, 0)
         if step == 1:
             forward_tokens()
         arrive(step, 1)
+        start_down(step)
         if step == 1:
             finish_tokens()
-
-    loads[2].wait()
-    pass_on(0, k, 2)
-    pass_on(1, k, 2)
-
-    tile = 2 * rows
-
-    @pl.loop(0, 4)
+            add_block(k, True)
+        for s in (k - step, k + step):
+            @pl.when((s >= 0) & (s < n))
+            def _():
+                add_block(s, False)
+
+    @pl.loop(0, 16)
     def _(i):
-        at = pl.ds(pl.multiple_of(i * tile, tile), tile)
-        both = jnp.dot(normed[at, :], gu[...], preferred_element_type=jnp.float32)
-        gate, up = both[:, :part], both[:, part:]
+        at = pl.ds(pl.multiple_of(i * (rows // 2), rows // 2), rows // 2)
+        gate, up = acc[at, :part], acc[at, part:]
         hidden[at, :] = (gate / (1.0 + jnp.exp(-gate)) * up).astype(jnp.bfloat16)
 
     mine = r * 2 + x
     others = ((r * 2 + (1 - x), along_x), (r_y * 2 + x, along_y), (r_y * 2 + (1 - x), diag))
 
-    def pair_copy(s):
+    def pair_copy(p):
         return pltpu.make_async_remote_copy(
-            pair_out.at[s], pair_in.at[s], pair_s.at[s], pair_r.at[s], device_id=partner, device_id_type=MESH
+            pair_out.at[p], pair_in.at[p], pair_s.at[p], pair_r.at[p], device_id=partner, device_id_type=MESH
         )
 
-    def cross_copy(s, to, where):
+    def cross_copy(p, to, where):
         return pltpu.make_async_remote_copy(
-            cross_out.at[s, to], cross_in.at[s, mine], cross_s.at[s, to], cross_r.at[s, mine],
+            cross_out.at[p, to], cross_in.at[p, mine], cross_s.at[p, to], cross_r.at[p, mine],
             device_id=where, device_id_type=MESH,
         )
 
-    def reduce_block(s):
+    both_ways = jnp.minimum(k, n - 1 - k)
+    far = jnp.where(k < n - 1 - k, 1, -1)
+
+    def source(i):
+        near = jnp.where(i % 2 == 1, k - (i + 1) // 2, k + i // 2)
+        return jnp.where(i <= 2 * both_ways, near, k + far * (i - both_ways))
+
+    def product(m, core, s, j):
+        at = pl.ds(pl.multiple_of((m * 2 + core) * rows, rows), rows)
+        return jnp.dot(hidden[at, :], dn[s, j], preferred_element_type=jnp.float32)
+
+    def finish(i, j, slot):
+        p = source(i) * cuts + j
+        pair_copy(p).wait_recv()
+        for to, where in (others[2], others[0], others[1]):
+            cross_out[p, to] = (kept[slot, to] + pair_in[p, to].astype(jnp.float32)).astype(jnp.bfloat16)
+        for to, where in (others[2], others[0], others[1]):
+            cross_copy(p, to, where).start()
+        fin[p] = kept[slot, mine] + pair_in[p, mine].astype(jnp.float32)
+
+    @pl.loop(0, n * cuts)
+    def _(at):
+        i, j, slot = at // cuts, at % cuts, at % 2
+        s = source(i)
+        p = s * cuts + j
+
+        @pl.when(i > 0)
+        def _():
+            remote(dn.at[s, j], w_s.at[0, s, 2 + j], w_r.at[s, 2 + j], partner).wait_recv()
+
+        @pl.when((i > 0) & (s < k))
+        def _():
+            pass_on(0, s, 2 + j)
+
+        @pl.when((i > 0) & (s > k))
+        def _():
+            pass_on(1, s, 2 + j)
+
         @pl.loop(0, 4)
         def _(m):
-            at = pl.ds(pl.multiple_of((m * 2 + (1 - c)) * rows, rows), rows)
-            pair_out[s, m] = jnp.dot(
-                hidden[at, :], dn[s], preferred_element_type=jnp.float32
-            ).astype(jnp.bfloat16)
-
-        pair_copy(s).start()
+            pair_out[p, m] = product(m, 1 - c, s, j).astype(jnp.bfloat16)
+
+        pair_copy(p).start()
 
         @pl.loop(0, 4)
         def _(m):
-            at = pl.ds(pl.multiple_of((m * 2 + c) * rows, rows), rows)
-            kept[m] = jnp.dot(hidden[at, :], dn[s], preferred_element_type=jnp.float32)
-
-        pair_copy(s).wait_recv()
-        for to, where in others:
-            cross_out[s, to] = (kept[to] + pair_in[s, to].astype(jnp.float32)).astype(jnp.bfloat16)
-        for to, where in (others[2], others[0], others[1]):
-            cross_copy(s, to, where).start()
-        fin[s] = kept[mine] + pair_in[s, mine].astype(jnp.float32)
-
-    reduce_block(k)
-    for step in range(1, n):
-        arrive(step, 2)
-        for s in (k - step, k + step):
-            @pl.when((s >= 0) & (s < n))
-            def _():
-                reduce_block(s)
-
-    def take(i):
-        for s_at in range(n):
-            for other, _ in others:
-                pltpu.make_async_remote_copy(
-                    cross_out.at[s_at, 0], cross_in.at[s_at, other], cross_s.at[s_at, 0],
-                    cross_r.at[s_at, other], device_id=along_x, device_id_type=MESH,
-                ).wait_recv()
-
-    take(0)
+            kept[slot, m] = product(m, c, s, j)
+
+        @pl.when(at > 0)
+        def _():
+            finish((at - 1) // cuts, (at - 1) % cuts, 1 - slot)
+
+    finish(n - 1, cuts - 1, (n * cuts - 1) % 2)
+
+    for p in range(n * cuts):
+        for other, _ in others:
+            pltpu.make_async_remote_copy(
+                cross_out.at[p, 0], cross_in.at[p, other], cross_s.at[p, 0],
+                cross_r.at[p, other], device_id=along_x, device_id_type=MESH,
+            ).wait_recv()
+
     piece = 32
 
     @pl.loop(0, rows // piece)
     def _(i):
         at = pl.ds(pl.multiple_of(i * piece, piece), piece)
         blocks = []
-        for s in range(n):
-            total = fin[s, at, :]
+        for p in range(n * cuts):
+            total = fin[p, at, :]
             for other, _ in others:
-                total = total + cross_in[s, other, at, :].astype(jnp.float32)
+                total = total + cross_in[p, other, at, :].astype(jnp.float32)
             blocks.append(total)
         square = sum(jnp.sum(b * b, axis=-1, keepdims=True) for b in blocks)
         scale = lax.rsqrt(square / (n * width) + EPS)
-        for s in range(n):
-            cols = pl.ds(s * width, width)
-            out_ref[at, cols] = (blocks[s] * scale * post_ref[:, cols]).astype(out_ref.dtype)
+        for p in range(n * cuts):
+            cols = pl.ds(p * sub, sub)
+            out_ref[at, cols] = (blocks[p] * scale * post_ref[:, cols]).astype(out_ref.dtype)
 
     for i in range(8):
         token_send(i).wait_send()
     for s in range(n):
-        for q in range(3):
+        for q in range(2 + cuts):
             @pl.when(has_right & (s <= k))
             def _():
                 hop(0, s, q).wait_send()
@@ -258,9 +307,10 @@
             @pl.when(has_left & (s >= k))
             def _():
                 hop(1, s, q).wait_send()
-        pair_copy(s).wait_send()
+    for p in range(n * cuts):
+        pair_copy(p).wait_send()
         for to, where in others:
-            cross_copy(s, to, where).wait_send()
+            cross_copy(p, to, where).wait_send()
 
 
 def chain_body(n, tokens, norm_gain, w_gate, w_up, w_down, post_gain):
@@ -268,36 +318,39 @@
     depth, block = w_gate.shape
     width = w_down.shape[1]
     part = block // 2
+    cuts = max(1, width // PIECE)
+    sub = width // cuts
     vmem, dma = pltpu.VMEM, pltpu.SemaphoreType.DMA
     low, full = jnp.bfloat16, jnp.float32
     anywhere = pl.BlockSpec(memory_space=pl.ANY)
     inside = pl.BlockSpec(memory_space=vmem)
     return pl.pallas_call(
-        functools.partial(kernel, n, rows, depth, part, width),
+        functools.partial(kernel, n, rows, depth, part, width, cuts),
         out_shape=jax.ShapeDtypeStruct((rows, model), low),
         in_specs=[anywhere, inside, anywhere, anywhere, anywhere, inside],
         out_specs=inside,
         scratch_shapes=[
             vmem((8 * rows, model), low),
             vmem((8 * rows, model), low),
-            vmem((n * depth, 2 * part), low),
-            vmem((n, part, width), low),
+            vmem((8 * rows, 2 * part), full),
+            vmem((n, depth, 2 * part), low),
+            vmem((n, cuts, part, sub), low),
             vmem((8 * rows, part), low),
-            vmem((4, rows, width), full),
-            vmem((n, 4, rows, width), low),
-            vmem((n, 4, rows, width), low),
-            vmem((n, 4, rows, width), low),
-            vmem((n, 4, rows, width), low),
-            vmem((n, rows, width), full),
-            dma((4,)),
+            vmem((2, 4, rows, sub), full),
+            vmem((n * cuts, 4, rows, sub), low),
+            vmem((n * cuts, 4, rows, sub), low),
+            vmem((n * cuts, 4, rows, sub), low),
+            vmem((n * cuts, 4, rows, sub), low),
+            vmem((n * cuts, rows, sub), full),
+            dma((3 + cuts,)),
             dma((8,)),
             dma((8,)),
-            dma((2, n, 3)),
-            dma((n, 3)),
-            dma((n,)),
-            dma((n,)),
-            dma((n, 4)),
-            dma((n, 4)),
+            dma((2, n, 2 + cuts)),
+            dma((n, 2 + cuts)),
+            dma((n * cuts,)),
+            dma((n * cuts,)),
+            dma((n * cuts, 4)),
+            dma((n * cuts, 4)),
         ],
         compiler_params=pltpu.CompilerParams(
             collective_id=0, has_side_effects=True, vmem_limit_bytes=56 * 2**20
@@ -313,7 +366,7 @@
         rows = tokens.shape[0]
         fits = (
             mesh.shape["rep"] == 2 and mesh.shape["tp"] == 4 and 2 <= n <= 4 and rows <= 128
-            and rows % 64 == 0 and w_gate.shape[1] % 256 == 0 and w_down.shape[1] % 128 == 0
+            and rows % 64 == 0 and w_gate.shape[1] % 256 == 0 and w_down.shape[1] % PIECE == 0
         )
         return chain_body(n, *args) if fits else plain_body(*args)
 

time: 96.8 us -> 95.7 us (0.989)
  Pallas kernels: 94.6 us -> 93.6 us
    pallas_call x1, Pallas kernels: 94.6 us -> 93.6 us  [chain_body(): pl.pallas_call(functools.partial(kernel, n, rows, depth, part, width, cut...]
where the time goes in v2:
time: 95.7 us; the launch traced here: 95.5 us
  Pallas kernels  93.6 us (98%)
  local copies, waits for them, and re-layouts  1.88 us (2%)
    pallas_call x1, Pallas kernels, chain_body(): pl.pallas_call(functools.partial(kernel, n, rows, depth, part, width, cut...  93.6 us

profile of v2, /device:TPU:0, one launch (start us, length us, event | category | flops | bytes accessed | tf_op | source)
XLA Modules:
  0.0 95.5 jit_solution(3063377445266168018)
XLA Ops:
  0.0 93.6 %shard_map.64 = bf16[128,2048]{1,0:T(8,128)(2,1)} custom-call(bf16[128,2048]{1,0:T(8,128)(2,1)} %tok_ref.1, f32[1,2048]{1,0:T(1,128)} %bitcast.2, bf16[512,768]{1,0:T(8,128)(2,1)} %wg_ref.1, bf16[512,768]{1,0:T(8,128)(2,1)} %wu_ref.1, bf16[768,512]{1,0:T(8,128)(2,1)} %wd_ref.1, f32[1,2048]{1,0:T(1,128)} %bitcast.3), custom_call_target="tpu_custom_call" | custom-call | tf_op jit(solution)/shard_map/pallas_call | solution.py:327
  93.6 1.9 %copy.8 = bf16[128,2048]{1,0:T(8,128)(2,1)} copy(bf16[128,2048]{1,0:T(8,128)(2,1)} %shard_map.64) | data formatting | bytes 1048576

commit v3 on v2

--- a/solution.py
+++ b/solution.py
@@ -244,6 +244,10 @@
         s = source(i)
         p = s * cuts + j
 
+        @pl.when(at > 0)
+        def _():
+            finish((at - 1) // cuts, (at - 1) % cuts, 1 - slot)
+
         @pl.when(i > 0)
         def _():
             remote(dn.at[s, j], w_s.at[0, s, 2 + j], w_r.at[s, 2 + j], partner).wait_recv()
@@ -265,10 +269,6 @@
         @pl.loop(0, 4)
         def _(m):
             kept[slot, m] = product(m, c, s, j)
-
-        @pl.when(at > 0)
-        def _():
-            finish((at - 1) // cuts, (at - 1) % cuts, 1 - slot)
 
     finish(n - 1, cuts - 1, (n * cuts - 1) % 2)
 

time: 95.7 us -> 94 us (0.982)
  Pallas kernels: 93.6 us -> 91.8 us
    pallas_call x1, Pallas kernels: 93.6 us -> 91.8 us  [chain_body(): pl.pallas_call(functools.partial(kernel, n, rows, depth, part, width, cut...]
where the time goes in v3:
time: 94 us; the launch traced here: 93.7 us
  Pallas kernels  91.8 us (98%)
  local copies, waits for them, and re-layouts  1.88 us (2%)
    pallas_call x1, Pallas kernels, chain_body(): pl.pallas_call(functools.partial(kernel, n, rows, depth, part, width, cut...  91.8 us
    unnamed x1, local copies, waits for them, and re-layouts  1.88 us

profile of v3, /device:TPU:0, one launch (start us, length us, event | category | flops | bytes accessed | tf_op | source)
XLA Modules:
  0.0 93.7 jit_solution(14161307211422612912)
XLA Ops:
  0.0 91.8 %shard_map.64 = bf16[128,2048]{1,0:T(8,128)(2,1)} custom-call(bf16[128,2048]{1,0:T(8,128)(2,1)} %tok_ref.1, f32[1,2048]{1,0:T(1,128)} %bitcast.2, bf16[512,768]{1,0:T(8,128)(2,1)} %wg_ref.1, bf16[512,768]{1,0:T(8,128)(2,1)} %wu_ref.1, bf16[768,512]{1,0:T(8,128)(2,1)} %wd_ref.1, f32[1,2048]{1,0:T(1,128)} %bitcast.3), custom_call_target="tpu_custom_call" | custom-call | tf_op jit(solution)/shard_map/pallas_call | solution.py:327
  91.8 1.9 %copy.8 = bf16[128,2048]{1,0:T(8,128)(2,1)} copy(bf16[128,2048]{1,0:T(8,128)(2,1)} %shard_map.64) | data formatting | bytes 1048576
